TPU v7x, 32 devices: a whole 2x2x4 slice. The times are simulated.
32 devices in a mesh: ep: 8 (over z, y), tp: 4 (over x, core).
Axes of the slice: x: 2, y: 2, z: 4, core: 2. Of those that a mesh axis runs over, the one named last changes fastest.
Arguments:
- mixer_in: bfloat16 [3072, 2048], P(('ep', 'tp')), may hold values from -6 to 6
- expert_in: bfloat16 [3072, 2048], P(('ep', 'tp')), may hold values from -6 to 6
- mixer_gain: float32 [2048], replicated, may hold values from 0.1 to 1.9
- in_gate_weight: bfloat16 [2048, 2048], P(None, 'tp'), may hold values from -0.125 to 0.125
- out_gate_weight: bfloat16 [2048, 2048], P(None, 'tp'), may hold values from -0.125 to 0.125
- value_weight: bfloat16 [2048, 2048], P(None, 'tp'), may hold values from -0.125 to 0.125
- conv_taps: float32 [3, 2048], replicated, may hold values from -3 to 3
- mixer_proj: bfloat16 [2048, 2048], P(None, 'tp'), may hold values from -0.125 to 0.125
- expert_gain: float32 [2048], replicated, may hold values from 0.1 to 1.9
- route_ids: int32 [3072, 2], P('ep'), may hold values from 0 to 7, all different within a row; in each aligned block of 96 rows (0 to 95, 96 to 191, ...) at most 48 rows name the same one
- route_weights: float32 [3072, 2], P('ep'), may hold values from 0.1 to 1
- gate_weight: bfloat16 [8, 2048, 1024], P('ep', None, 'tp'), may hold values from -0.125 to 0.125
- up_weight: bfloat16 [8, 2048, 1024], P('ep', None, 'tp'), may hold values from -0.125 to 0.125
- down_weight: bfloat16 [8, 1024, 2048], P('ep', None, 'tp'), may hold values from -0.1875 to 0.1875
Outputs:
- mixer_out: bfloat16 [3072, 2048], P('ep', 'tp')
- expert_out: bfloat16 [3072, 2048], P('ep', 'tp')
Inputs may be any that keep to these rules, and one draw needn't show every extreme that they name: `route_ids`: each row names 2 different experts. In each aligned block of 96 rows no expert is named by more than 48 rows, a bound that some block reaches.
All inputs are finite; a program needn't handle non-finite values.
Results may differ from a plain program's by a relative error of at most 0.0076.
Values may be sent and summed in bfloat16 or wider, within the bound.
No kernel may reach another device: no remote copies, remote signals or barrier semaphores. Data moves between devices by JAX's collectives and lax.ppermute only.
A program may use at most 64 MiB of HBM per device.

v0:
```python
import jax
import jax.numpy as jnp
from jax import lax
from jax.sharding import PartitionSpec as P

norm_eps = 1e-06


def passed_along(value, axis, steps):
    count = lax.axis_size(axis)
    leading, last = (max(0, -steps), min(count, count - steps))
    return lax.ppermute(value, axis, [(source, source + steps) for source in range(leading, last)])


def rms_rows(values, gain_row):
    wide = values.astype(jnp.float32)
    scale = lax.rsqrt(jnp.mean(wide * wide, axis=-1, keepdims=True) + norm_eps)
    return (wide * scale * gain_row).astype(jnp.bfloat16)


def place_slots(route_ids, group_rows, experts, slot_cap):
    row_total, top_count = route_ids.shape
    groups = row_total // group_rows
    labels = jnp.arange(experts, dtype=jnp.int32)
    onehot = (
        route_ids.reshape(groups, group_rows * top_count)[:, :, None] == labels[None, None, :]
    ).astype(jnp.int32)
    earlier = jnp.cumsum(onehot, axis=1) - onehot
    within = jnp.sum(earlier * onehot, axis=2)
    slot_index = jnp.arange(groups, dtype=jnp.int32)[:, None] * slot_cap + within
    return slot_index.reshape(row_total, top_count)


def on_device(
    mixer_in,
    expert_in,
    mixer_gain,
    in_gate_weight,
    out_gate_weight,
    value_weight,
    conv_taps,
    mixer_proj,
    expert_gain,
    route_ids,
    route_weights,
    gate_weight,
    up_weight,
    down_weight,
):
    tok_dev = mixer_in.shape[0]
    tp_count = lax.axis_size("tp")
    ep_count = lax.axis_size("ep")
    top_count = route_ids.shape[1]
    experts = ep_count * gate_weight.shape[0]
    slot_cap = max(2, 2 * tok_dev * top_count // experts)
    tp_index = lax.axis_index("tp")
    mixer_normed = rms_rows(mixer_in, mixer_gain)
    expert_normed = rms_rows(expert_in, expert_gain)
    block_slot = place_slots(route_ids, tok_dev, experts, slot_cap)
    mixer_rows = lax.all_gather(mixer_normed, "tp", axis=0, tiled=True)
    send_ids = lax.dynamic_slice_in_dim(route_ids, tp_index * tok_dev, tok_dev, 0)
    send_slot = (
        lax.dynamic_slice_in_dim(block_slot, tp_index * tok_dev, tok_dev, 0) - tp_index * slot_cap
    )
    source_count = expert_normed.shape[0]
    flat_index = (send_ids * slot_cap + send_slot).reshape(-1)
    row_table = (
        jnp.full((experts * slot_cap,), source_count, jnp.int32)
        .at[flat_index]
        .set(jnp.repeat(jnp.arange(source_count, dtype=jnp.int32), top_count))
    )
    padded_rows = jnp.concatenate(
        [expert_normed, jnp.zeros((1, expert_normed.shape[1]), jnp.bfloat16)], axis=0
    )
    outgoing = padded_rows[row_table].reshape(experts, slot_cap, expert_normed.shape[1])
    arrived = lax.all_to_all(outgoing, "ep", split_axis=0, concat_axis=0, tiled=True)
    arrived = lax.all_gather(arrived, "tp", axis=1, tiled=True)
    chan_width = in_gate_weight.shape[1]
    in_gate = jnp.dot(mixer_rows, in_gate_weight, preferred_element_type=jnp.float32)
    out_gate = jnp.dot(mixer_rows, out_gate_weight, preferred_element_type=jnp.float32)
    values = jnp.dot(mixer_rows, value_weight, preferred_element_type=jnp.float32)
    product = (in_gate * values).astype(jnp.bfloat16)
    tap_count = conv_taps.shape[0]
    rim_rows = passed_along(product[product.shape[0] - (tap_count - 1) :], "ep", 1)
    extended = jnp.concatenate([rim_rows, product], axis=0).astype(jnp.float32)
    tap_rows = lax.dynamic_slice_in_dim(conv_taps, tp_index * chan_width, chan_width, 1)
    row_count = product.shape[0]
    conv_sum = tap_rows[0] * extended[0:row_count]
    for tap_index in range(1, tap_count):
        conv_sum = conv_sum + tap_rows[tap_index] * extended[tap_index : tap_index + row_count]
    gated = (out_gate * conv_sum).astype(jnp.bfloat16)
    slots_in = arrived.reshape(-1, arrived.shape[2])
    gate_pre = jnp.dot(slots_in, gate_weight[0], preferred_element_type=jnp.float32)
    up_pre = jnp.dot(slots_in, up_weight[0], preferred_element_type=jnp.float32)
    hidden = (jax.nn.silu(gate_pre) * up_pre).astype(jnp.bfloat16)
    down_slice = down_weight[0]
    gated_all, hidden_all = (
        lax.all_gather(gated, "tp", axis=1, tiled=True),
        lax.all_gather(hidden, "tp", axis=1, tiled=True),
    )
    mixer_sum = jnp.dot(gated_all, mixer_proj, preferred_element_type=jnp.float32)
    expert_sum = jnp.dot(hidden_all, down_slice, preferred_element_type=jnp.float32)
    mixer_out = mixer_sum.astype(jnp.bfloat16)
    results = expert_sum.astype(jnp.bfloat16).reshape(ep_count, -1, expert_sum.shape[1])
    returned = lax.all_to_all(results, "ep", split_axis=0, concat_axis=0, tiled=True)
    back_index = (route_ids * (tp_count * slot_cap) + block_slot).reshape(-1)
    picked = returned.reshape(-1, returned.shape[2])[back_index].reshape(
        route_ids.shape[0], top_count, -1
    )
    shares = route_weights / jnp.sum(route_weights, axis=1, keepdims=True)
    expert_out = jnp.sum(picked.astype(jnp.float32) * shares[:, :, None], axis=1).astype(
        jnp.bfloat16
    )
    return (mixer_out, expert_out)


def solution(mesh):
    return jax.shard_map(
        on_device,
        mesh=mesh,
        in_specs=(
            P(("ep", "tp"), None),
            P(("ep", "tp"), None),
            P(),
            P(None, "tp"),
            P(None, "tp"),
            P(None, "tp"),
            P(),
            P(None, "tp"),
            P(),
            P("ep", None),
            P("ep", None),
            P("ep", None, "tp"),
            P("ep", None, "tp"),
            P("ep", None, "tp"),
        ),
        out_specs=(P("ep", "tp"), P("ep", "tp")),
        check_vma=False,
    )
```

profile of v0, /device:TPU:0, one launch (start us, length us, event | category | flops | bytes accessed | tf_op | source)
XLA Modules:
  0.0 225.8 jit_solution(8903931806457454474)
XLA Ops:
  7.3 1.0 copy.26
  8.4 2.3 %reduce-window.6 = s32[4,8,2,128]{3,1,2,0:T(8,128)S(1)} reduce-window(s32[4,8,2,128]{3,1,2,0:T(8,128)S(1)} %convert_bitcast_fusion, s32[]{:T(128)} %constant.19.clone.1), window={size=1x1x1x128 pad=0_0x0_0x0_0x127_0}, to_apply=%region_2.0 | reduce-window | flops 1040384 | bytes 65540 | tf_op jit(solution)/shard_map/reduce-window
  13.3 1.2 scatter_custom_fusion
  15.0 3.1 %gather_fusion = bf16[384,2048]{1,0:T(8,128)(2,1)} fusion(bf16[97,2048]{1,0:T(8,128)(2,1)S(1)} %concatenate.7, s32[1024]{0:T(1024)S(1)} %pad_clamp_fusion.1), kind=kCustom, calls=%fused_computation | custom fusion | bytes 3147264 | tf_op jit(solution)/shard_map/gather | solution.py:75
  18.1 44.4 %all_to_all.10 = bf16[8,48,2048]{2,1,0:T(8,128)(2,1)} all-to-all(bf16[8,48,2048]{2,1,0:T(8,128)(2,1)} %bitcast.37), channel_id=1, replica_groups=mesh['ep'=8,'tp'=4] {'ep'}, dimensions={0} | all-to-all | bytes 3145728 | tf_op jit(solution)/shard_map/all_to_all | solution.py:76
  62.6 0.9 copy-done.2
  63.7 0.9 fusion.9
  64.7 43.4 %all-gather.9.cloned.1.call-done = bf16[8,192,2048]{2,1,0:T(8,128)(2,1)} async-done(((bf16[8,48,2048]{2,1,0:T(8,128)(2,1)}), bf16[8,192,2048]{2,1,0:T(8,128)(2,1)}) %all-gather.9.cloned.1.call-update) | async-done | bytes 6291472 | tf_op jit(solution)/shard_map/all_gather | solution.py:77
  108.1 4.8 %fusion.5 = f32[1536,256]{1,0:T(8,128)S(1)} fusion(bf16[1536,2048]{1,0:T(8,128)(2,1)} %bitcast.43, bf16[1,2048,256]{2,1,0:T(8,128)(2,1)S(1)} %copy-done.9), kind=kOutput, calls=%fused_computation.14 | convolution fusion | flops 1610612736 | bytes 8912896 | tf_op jit(solution)/shard_map/dot_general | solution.py:93
  112.9 3.0 %fusion = bf16[1536,256]{1,0:T(8,128)(2,1)} fusion(bf16[1536,2048]{1,0:T(8,128)(2,1)S(1)} %bitcast.44, f32[1536,256]{1,0:T(8,128)S(1)} %fusion.5, bf16[1,2048,256]{2,1,0:T(8,128)(2,1)S(1)} %copy-done.10), kind=kOutput, calls=%fused_computation.5 | convolution fusion | flops 1612972032 | bytes 9699328 | tf_op jit(solution)/shard_map/dot_general | solution.py:94
  115.9 14.0 %all-gather.5.cloned.1.call-done = bf16[384,2048]{1,0:T(8,128)(2,1)} async-done(((bf16[96,2048]{1,0:T(8,128)(2,1)}), bf16[384,2048]{1,0:T(8,128)(2,1)}) %all-gather.5.cloned.1.call-update) | async-done | bytes 1572880 | tf_op jit(solution)/shard_map/all_gather | solution.py:60
  129.9 2.5 %fusion.22 = f32[384,512]{1,0:T(8,128)S(1)} fusion(bf16[384,2048]{1,0:T(8,128)(2,1)} %all-gather.5.cloned.1.call-done, bf16[2048,512]{1,0:T(8,128)(2,1)S(1)} %copy-done), kind=kOutput, calls=%fused_computation.57 | convolution fusion | flops 805306368 | bytes 4456448 | tf_op jit(solution)/shard_map/dot_general | solution.py:79
  132.4 1.0 fusion.2
  133.4 3.4 %collective-permute-start = (bf16[2,512]{1,0:T(2,128)(2,1)S(1)}, bf16[2,512]{1,0:T(2,128)(2,1)S(1)}, u32[]{:S(2)}, u32[]{:S(2)}) collective-permute-start(bf16[2,512]{1,0:T(2,128)(2,1)S(1)} %slice.44), channel_id=1, source_target_pairs={{0,4},{4,8},{8,12},{12,16},{16,20},{20,24},{24,28},{1,5},{5,9},{9,... | collective-permute-start | bytes 6152 | tf_op jit(solution)/shard_map/ppermute | solution.py:12
  138.2 22.1 %all-gather.11.cloned.1.call-done = bf16[1536,1024]{1,0:T(8,128)(2,1)} async-done(((bf16[1536,256]{1,0:T(8,128)(2,1)}), bf16[1536,1024]{1,0:T(8,128)(2,1)}) %all-gather.11.cloned.1.call-update) | async-done | bytes 3145744 | tf_op jit(solution)/shard_map/all_gather | solution.py:99
  160.3 5.1 %convolution_convert_fusion = bf16[1536,512]{1,0:T(8,128)(2,1)} fusion(bf16[1536,1024]{1,0:T(8,128)(2,1)} %all-gather.11.cloned.1.call-done, bf16[1,1024,512]{2,1,0:T(8,128)(2,1)} %param.27), kind=kOutput, calls=%fused_computation.3 | convolution fusion | flops 1611399168 | bytes 5767168 | tf_op jit(solution)/shard_map/dot_general | solution.py:102
  165.5 5.5 %all-to-all-start.1 = ((bf16[8,192,512]{2,1,0:T(8,128)(2,1)}), bf16[8,192,512]{2,1,0:T(8,128)(2,1)}, u32[]{:S(2)}, u32[]{:S(2)}) async-start(bf16[8,192,512]{2,1,0:T(8,128)(2,1)} %bitcast.38), calls=%async_computation.1 | async-start | bytes 3145728 | tf_op jit(solution)/shard_map/all_to_all | solution.py:105
  171.2 3.9 %fusion.1 = bf16[384,512]{1,0:T(8,128)(2,1)} fusion(bf16[384,2048]{1,0:T(8,128)(2,1)} %all-gather.5.cloned.1.call-done, bf16[2048,512]{1,0:T(8,128)(2,1)} %param.18, f32[386,512]{1,0:T(8,128)S(1)} %maximum_convert_fusion, f32[512]{0:T(512)S(1)} %bitcast.41, f32[512]{0:T(512)S(1)} %bitcast.40, f32[512]{0:T(512)S(1)} %bitcast.39), kind=kOutput, calls=%fused_computation.9 | convolution fusion | flops 806682624 | bytes 6428672 | tf_op jit(solution)/shard_map/dot_general | solution.py:80
  175.7 19.5 %all-gather.7.cloned.1.call-done = bf16[384,2048]{1,0:T(8,128)(2,1)} async-done(((bf16[384,512]{1,0:T(8,128)(2,1)}), bf16[384,2048]{1,0:T(8,128)(2,1)}) %all-gather.7.cloned.1.call-update) | async-done | bytes 1572880 | tf_op jit(solution)/shard_map/all_gather | solution.py:98
  195.2 3.8 %convolution_convert_fusion.1 = bf16[384,512]{1,0:T(8,128)(2,1)} fusion(bf16[384,2048]{1,0:T(8,128)(2,1)} %all-gather.7.cloned.1.call-done, bf16[2048,512]{1,0:T(8,128)(2,1)} %param.21), kind=kOutput, calls=%fused_computation.11 | convolution fusion | flops 805502976 | bytes 4063232 | tf_op jit(solution)/shard_map/dot_general | solution.py:101
  199.0 9.5 %all-to-all-done.1 = bf16[8,192,512]{2,1,0:T(8,128)(2,1)} async-done(((bf16[8,192,512]{2,1,0:T(8,128)(2,1)}), bf16[8,192,512]{2,1,0:T(8,128)(2,1)}, u32[]{:S(2)}, u32[]{:S(2)}) %all-to-all-start.1) | async-done | bytes 1572896 | tf_op jit(solution)/shard_map/all_to_all | solution.py:105
  208.5 4.3 %gather_fusion.1 = bf16[768,512]{1,0:T(8,128)(2,1)S(1)} fusion(bf16[1536,512]{1,0:T(8,128)(2,1)} %bitcast.14, s32[1024]{0:T(1024)S(1)} %pad_clamp_fusion), kind=kCustom, calls=%fused_computation.1 | custom fusion | bytes 1575936 | tf_op jit(solution)/shard_map/gather | solution.py:107
  212.8 2.1 reshape.134
  215.0 4.3 %multiply_reduce_fusion = bf16[384,512]{1,0:T(8,128)(2,1)} fusion(f32[384,2,512]{2,1,0:T(2,128)} %reshape.134, f32[384,2]{1,0:T(8,128)S(1)} %copy.32), kind=kLoop, calls=%fused_computation.6 | loop fusion | flops 589824 | bytes 1969152 | tf_op jit(solution)/shard_map/reduce_sum | solution.py:111
  (70 shorter events, 5.7 us)
Async XLA Ops:
  7.2 122.7 %copy-start = (bf16[2048,512]{1,0:T(8,128)(2,1)S(1)}, bf16[2048,512]{1,0:T(8,128)(2,1)}, u32[]{:S(2)}) copy-start(bf16[2048,512]{1,0:T(8,128)(2,1)} %param.17) | copy-start | bytes 6291460
  7.2 7.4 %copy-start.1 = (bf16[96,2048]{1,0:T(8,128)(2,1)S(1)}, bf16[96,2048]{1,0:T(8,128)(2,1)}, u32[]{:S(2)}) copy-start(bf16[96,2048]{1,0:T(8,128)(2,1)} %param.15) | copy-start | bytes 1179652
  7.2 7.6 %copy-start.4 = (f32[2048]{0:T(1024)S(1)}, f32[2048]{0:T(1024)}, u32[]{:S(2)}) copy-start(f32[2048]{0:T(1024)} %param.22) | copy-start | bytes 24580
  7.2 100.8 %all-gather.9.cloned.1.call-start = ((), (), s32[]{:S(2)}) async-start(), calls=%async_computation.4 | async-start | bytes 7864320 | tf_op jit(solution)/shard_map/all_gather | solution.py:77
  62.5 1.0 copy-start.2
  62.5 1.2 copy-start.5
  62.5 45.5 %copy-start.9 = (bf16[1,2048,256]{2,1,0:T(8,128)(2,1)S(1)}, bf16[1,2048,256]{2,1,0:T(8,128)(2,1)}, u32[]{:S(2)}) copy-start(bf16[1,2048,256]{2,1,0:T(8,128)(2,1)} %param.25) | copy-start | bytes 3145732
  62.5 67.3 %all-gather.5.cloned.1.call-start = ((), (), s32[]{:S(2)}) async-start(), calls=%async_computation.2 | async-start | bytes 1966080 | tf_op jit(solution)/shard_map/all_gather | solution.py:60
  64.6 95.7 %all-gather.11.cloned.1.call-start = ((), (), s32[]{:S(2)}) async-start(), calls=%async_computation.5 | async-start | bytes 3932160 | tf_op jit(solution)/shard_map/all_gather | solution.py:99
  108.0 4.8 %copy-start.6 = (bf16[8,192,2048]{2,1,0:T(8,128)(2,1)S(1)}, bf16[8,192,2048]{2,1,0:T(8,128)(2,1)}, u32[]{:S(2)}) copy-start(bf16[8,192,2048]{2,1,0:T(8,128)(2,1)} %all-gather.9.cloned.1.call-done) | copy-start | bytes 18874372
  108.1 4.9 %copy-start.10 = (bf16[1,2048,256]{2,1,0:T(8,128)(2,1)S(1)}, bf16[1,2048,256]{2,1,0:T(8,128)(2,1)}, u32[]{:S(2)}) copy-start(bf16[1,2048,256]{2,1,0:T(8,128)(2,1)} %param.26) | copy-start | bytes 3145732
  129.8 2.5 %copy-start.7 = (bf16[2048,512]{1,0:T(8,128)(2,1)S(1)}, bf16[2048,512]{1,0:T(8,128)(2,1)}, u32[]{:S(2)}) copy-start(bf16[2048,512]{1,0:T(8,128)(2,1)} %param.19) | copy-start | bytes 6291460
  129.9 2.5 %copy-start.8 = (bf16[384,2048]{1,0:T(8,128)(2,1)S(1)}, bf16[384,2048]{1,0:T(8,128)(2,1)}, u32[]{:S(2)}) copy-start(bf16[384,2048]{1,0:T(8,128)(2,1)} %all-gather.5.cloned.1.call-done) | copy-start | bytes 4718596
  133.4 4.7 %collective-permute-start = (bf16[2,512]{1,0:T(2,128)(2,1)S(1)}, bf16[2,512]{1,0:T(2,128)(2,1)S(1)}, u32[]{:S(2)}, u32[]{:S(2)}) collective-permute-start(bf16[2,512]{1,0:T(2,128)(2,1)S(1)} %slice.44), channel_id=1, source_target_pairs={{0,4},{4,8},{8,12},{12,16},{16,20},{20,24},{24,28},{1,5},{5,9},{9,... | collective-permute-start | bytes 6152 | tf_op jit(solution)/shard_map/ppermute | solution.py:12
  165.5 43.0 %all-to-all-start.1 = ((bf16[8,192,512]{2,1,0:T(8,128)(2,1)}), bf16[8,192,512]{2,1,0:T(8,128)(2,1)}, u32[]{:S(2)}, u32[]{:S(2)}) async-start(bf16[8,192,512]{2,1,0:T(8,128)(2,1)} %bitcast.38), calls=%async_computation.1 | async-start | bytes 3145728 | tf_op jit(solution)/shard_map/all_to_all | solution.py:105
  171.0 24.2 %all-gather.7.cloned.1.call-start = ((), (), s32[]{:S(2)}) async-start(), calls=%async_computation.3 | async-start | bytes 1966080 | tf_op jit(solution)/shard_map/all_gather | solution.py:98
  171.2 4.2 %copy-start.3 = (f32[384,2]{0,1:T(2,128)S(1)}, f32[384,2]{0,1:T(2,128)}, u32[]{:S(2)}) copy-start(f32[384,2]{0,1:T(2,128)} %param.24) | copy-start | bytes 9220
Sparse Core Ops, SparseCore 0:
  62.7 45.3 all-gather.8
  110.2 19.6 all-gather.4
  131.4 28.8 all-gather.10
  175.3 19.8 all-gather.6
where the time goes:
time: 226 us
  waiting for transfers between devices  109 us (48%)
  blocking collectives  44.4 us (20%)
  matrix products  24.1 us (11%)
  local copies, waits for them, and re-layouts  15.3 us (7%)
  between operations  14 us (6%)
  other arithmetic  9.84 us (4%)
  starting transfers between devices  9.23 us (4%)
    all_to_all x1, blocking collectives, on_device(): lax.all_to_all(outgoing, 'ep', split_axis=0, concat_axis=0, tiled=True)  44.4 us
    all_gather x1, waiting for transfers between devices, on_device(): arrived = lax.all_gather(arrived, 'tp', axis=1, tiled=True)  43.4 us
    all_gather x1, waiting for transfers between devices, on_device(): lax.all_gather(hidden, 'tp', axis=1, tiled=True)  22.1 us
    all_gather x1, waiting for transfers between devices, on_device(): lax.all_gather(gated, 'tp', axis=1, tiled=True)  19.5 us
    all_gather x1, waiting for transfers between devices, on_device(): mixer_rows = lax.all_gather(mixer_normed, 'tp', axis=0, tiled=True)  14 us
    all_to_all x1, waiting for transfers between devices, on_device(): lax.all_to_all(results, 'ep', split_axis=0, concat_axis=0, tiled=True)  9.53 us
    all_to_all x1, starting transfers between devices, on_device(): lax.all_to_all(results, 'ep', split_axis=0, concat_axis=0, tiled=True)  5.52 us
    dot_general x1, matrix products, on_device(): jnp.dot(hidden_all, down_slice, preferred_element_type=jnp.float32)  5.13 us
  transfers between devices with their start and end apart: 6, of which 6 were waited for; matrix products, arithmetic and copies ran while one was open for 10% of the time, Pallas kernels for 0%

commit v1 on v0

--- a/solution.py
+++ b/solution.py
@@ -74,7 +74,8 @@
     )
     outgoing = padded_rows[row_table].reshape(experts, slot_cap, expert_normed.shape[1])
     arrived = lax.all_to_all(outgoing, "ep", split_axis=0, concat_axis=0, tiled=True)
-    arrived = lax.all_gather(arrived, "tp", axis=1, tiled=True)
+    terms = lax.all_gather(arrived, "tp", axis=0, tiled=False)
+    arrived = jnp.concatenate(terms, axis=1)
     chan_width = in_gate_weight.shape[1]
     in_gate = jnp.dot(mixer_rows, in_gate_weight, preferred_element_type=jnp.float32)
     out_gate = jnp.dot(mixer_rows, out_gate_weight, preferred_element_type=jnp.float32)

time: 226 us -> 226 us (level)
  local copies, waits for them, and re-layouts: 15.3 us -> 18.7 us
  matrix products: 24.1 us -> 21.2 us
    reshape x0 -> x1, local copies, waits for them, and re-layouts: none -> 3.45 us  [on_device(): arrived = jnp.concatenate(terms, axis=1)]
    dot_general x1, matrix products: 4.78 us -> 1.91 us  [on_device(): jnp.dot(slots_in, gate_weight[0], preferred_element_type=jnp.float32)]
where the time goes in v1:
time: 226 us
  waiting for transfers between devices  108 us (48%)
  blocking collectives  44.4 us (20%)
  matrix products  21.2 us (9%)
  local copies, waits for them, and re-layouts  18.7 us (8%)
  between operations  14.1 us (6%)
  other arithmetic  9.84 us (4%)
  starting transfers between devices  9.23 us (4%)
    all_to_all x1, blocking collectives, on_device(): lax.all_to_all(outgoing, 'ep', split_axis=0, concat_axis=0, tiled=True)  44.4 us
    all_gather x1, waiting for transfers between devices, on_device(): terms = lax.all_gather(arrived, 'tp', axis=0, tiled=False)  43.4 us
    all_gather x1, waiting for transfers between devices, on_device(): lax.all_gather(hidden, 'tp', axis=1, tiled=True)  22.1 us
    all_gather x1, waiting for transfers between devices, on_device(): lax.all_gather(gated, 'tp', axis=1, tiled=True)  19.5 us
    all_gather x1, waiting for transfers between devices, on_device(): mixer_rows = lax.all_gather(mixer_normed, 'tp', axis=0, tiled=True)  13.4 us
    all_to_all x1, waiting for transfers between devices, on_device(): lax.all_to_all(results, 'ep', split_axis=0, concat_axis=0, tiled=True)  9.53 us
    all_to_all x1, starting transfers between devices, on_device(): lax.all_to_all(results, 'ep', split_axis=0, concat_axis=0, tiled=True)  5.52 us
    dot_general x1, matrix products, on_device(): jnp.dot(hidden_all, down_slice, preferred_element_type=jnp.float32)  5.12 us
  transfers between devices with their start and end apart: 6, of which 6 were waited for; matrix products, arithmetic and copies ran while one was open for 10% of the time, Pallas kernels for 0%

profile of v1, /device:TPU:0, one launch (start us, length us, event | category | flops | bytes accessed | tf_op | source)
XLA Modules:
  0.0 225.8 jit_solution(11423715341642668984)
XLA Ops:
  7.3 1.0 copy.42
  8.4 2.3 %reduce-window.6 = s32[4,8,2,128]{3,1,2,0:T(8,128)S(1)} reduce-window(s32[4,8,2,128]{3,1,2,0:T(8,128)S(1)} %convert_bitcast_fusion, s32[]{:T(128)} %constant.19.clone.1), window={size=1x1x1x128 pad=0_0x0_0x0_0x127_0}, to_apply=%region_2.0 | reduce-window | flops 1040384 | bytes 65540 | tf_op jit(solution)/shard_map/reduce-window
  13.3 1.2 scatter_custom_fusion
  15.0 3.1 %gather_fusion = bf16[384,2048]{1,0:T(8,128)(2,1)} fusion(bf16[97,2048]{1,0:T(8,128)(2,1)S(1)} %concatenate.7, s32[1024]{0:T(1024)S(1)} %pad_clamp_fusion.1), kind=kCustom, calls=%fused_computation | custom fusion | bytes 3147264 | tf_op jit(solution)/shard_map/gather | solution.py:75
  18.1 44.4 %all_to_all.10 = bf16[8,48,2048]{2,1,0:T(8,128)(2,1)} all-to-all(bf16[8,48,2048]{2,1,0:T(8,128)(2,1)} %bitcast.43), channel_id=1, replica_groups=mesh['ep'=8,'tp'=4] {'ep'}, dimensions={0} | all-to-all | bytes 3145728 | tf_op jit(solution)/shard_map/all_to_all | solution.py:76
  62.6 0.9 copy-done.2
  64.7 43.4 %all-gather.12.cloned.1.call-done = bf16[32,48,2048]{2,1,0:T(8,128)(2,1)} async-done(((bf16[8,48,2048]{2,1,0:T(8,128)(2,1)}), bf16[32,48,2048]{2,1,0:T(8,128)(2,1)}) %all-gather.12.cloned.1.call-update) | async-done | bytes 6291472 | tf_op jit(solution)/shard_map/all_gather | solution.py:77
  108.1 3.5 %copy.47 = bf16[8,4,48,2048]{3,2,1,0:T(8,128)(2,1)S(1)} copy(bf16[8,4,48,2048]{3,2,0,1:T(8,128)(2,1)} %bitcast.40) | data formatting | bytes 12582912 | tf_op jit(solution)/shard_map/reshape | solution.py:78
  111.5 1.9 fusion.5
  113.5 3.0 %fusion = bf16[1536,256]{1,0:T(8,128)(2,1)} fusion(bf16[1536,2048]{1,0:T(8,128)(2,1)S(1)} %bitcast.42, f32[1536,256]{1,0:T(8,128)S(1)} %fusion.5, bf16[1,2048,256]{2,1,0:T(8,128)(2,1)S(1)} %copy-done.9), kind=kOutput, calls=%fused_computation.5 | convolution fusion | flops 1612972032 | bytes 9699328 | tf_op jit(solution)/shard_map/dot_general | solution.py:95
  116.5 13.4 %all-gather.6.cloned.1.call-done = bf16[384,2048]{1,0:T(8,128)(2,1)} async-done(((bf16[96,2048]{1,0:T(8,128)(2,1)}), bf16[384,2048]{1,0:T(8,128)(2,1)}) %all-gather.6.cloned.1.call-update) | async-done | bytes 1572880 | tf_op jit(solution)/shard_map/all_gather | solution.py:60
  129.9 2.5 %fusion.22 = f32[384,512]{1,0:T(8,128)S(1)} fusion(bf16[384,2048]{1,0:T(8,128)(2,1)} %all-gather.6.cloned.1.call-done, bf16[2048,512]{1,0:T(8,128)(2,1)S(1)} %copy-done), kind=kOutput, calls=%fused_computation.57 | convolution fusion | flops 805306368 | bytes 4456448 | tf_op jit(solution)/shard_map/dot_general | solution.py:80
  132.4 1.0 fusion.2
  133.4 3.4 %collective-permute-start = (bf16[2,512]{1,0:T(2,128)(2,1)S(1)}, bf16[2,512]{1,0:T(2,128)(2,1)S(1)}, u32[]{:S(2)}, u32[]{:S(2)}) collective-permute-start(bf16[2,512]{1,0:T(2,128)(2,1)S(1)} %slice.44), channel_id=1, source_target_pairs={{0,4},{4,8},{8,12},{12,16},{16,20},{20,24},{24,28},{1,5},{5,9},{9,... | collective-permute-start | bytes 6152 | tf_op jit(solution)/shard_map/ppermute | solution.py:12
  138.2 22.1 %all-gather.10.cloned.1.call-done = bf16[1536,1024]{1,0:T(8,128)(2,1)} async-done(((bf16[1536,256]{1,0:T(8,128)(2,1)}), bf16[1536,1024]{1,0:T(8,128)(2,1)}) %all-gather.10.cloned.1.call-update) | async-done | bytes 3145744 | tf_op jit(solution)/shard_map/all_gather | solution.py:100
  160.3 5.1 %convolution_convert_fusion = bf16[1536,512]{1,0:T(8,128)(2,1)} fusion(bf16[1536,1024]{1,0:T(8,128)(2,1)} %all-gather.10.cloned.1.call-done, bf16[1,1024,512]{2,1,0:T(8,128)(2,1)} %param.27), kind=kOutput, calls=%fused_computation.3 | convolution fusion | flops 1611399168 | bytes 5767168 | tf_op jit(solution)/shard_map/dot_general | solution.py:103
  165.5 5.5 %all-to-all-start.1 = ((bf16[8,192,512]{2,1,0:T(8,128)(2,1)}), bf16[8,192,512]{2,1,0:T(8,128)(2,1)}, u32[]{:S(2)}, u32[]{:S(2)}) async-start(bf16[8,192,512]{2,1,0:T(8,128)(2,1)} %bitcast.44), calls=%async_computation.1 | async-start | bytes 3145728 | tf_op jit(solution)/shard_map/all_to_all | solution.py:106
  171.2 3.9 %fusion.1 = bf16[384,512]{1,0:T(8,128)(2,1)} fusion(bf16[384,2048]{1,0:T(8,128)(2,1)} %all-gather.6.cloned.1.call-done, bf16[2048,512]{1,0:T(8,128)(2,1)} %param.18, f32[386,512]{1,0:T(8,128)S(1)} %maximum_convert_fusion, f32[512]{0:T(512)S(1)} %bitcast.47, f32[512]{0:T(512)S(1)} %bitcast.46, f32[512]{0:T(512)S(1)} %bitcast.45), kind=kOutput, calls=%fused_computation.9 | convolution fusion | flops 806682624 | bytes 6428672 | tf_op jit(solution)/shard_map/dot_general | solution.py:81
  175.7 19.5 %all-gather.8.cloned.1.call-done = bf16[384,2048]{1,0:T(8,128)(2,1)} async-done(((bf16[384,512]{1,0:T(8,128)(2,1)}), bf16[384,2048]{1,0:T(8,128)(2,1)}) %all-gather.8.cloned.1.call-update) | async-done | bytes 1572880 | tf_op jit(solution)/shard_map/all_gather | solution.py:99
  195.2 3.8 %convolution_convert_fusion.1 = bf16[384,512]{1,0:T(8,128)(2,1)} fusion(bf16[384,2048]{1,0:T(8,128)(2,1)} %all-gather.8.cloned.1.call-done, bf16[2048,512]{1,0:T(8,128)(2,1)} %param.21), kind=kOutput, calls=%fused_computation.11 | convolution fusion | flops 805502976 | bytes 4063232 | tf_op jit(solution)/shard_map/dot_general | solution.py:102
  199.0 9.5 %all-to-all-done.1 = bf16[8,192,512]{2,1,0:T(8,128)(2,1)} async-done(((bf16[8,192,512]{2,1,0:T(8,128)(2,1)}), bf16[8,192,512]{2,1,0:T(8,128)(2,1)}, u32[]{:S(2)}, u32[]{:S(2)}) %all-to-all-start.1) | async-done | bytes 1572896 | tf_op jit(solution)/shard_map/all_to_all | solution.py:106
  208.5 4.3 %gather_fusion.1 = bf16[768,512]{1,0:T(8,128)(2,1)S(1)} fusion(bf16[1536,512]{1,0:T(8,128)(2,1)} %bitcast.16, s32[1024]{0:T(1024)S(1)} %pad_clamp_fusion), kind=kCustom, calls=%fused_computation.1 | custom fusion | bytes 1575936 | tf_op jit(solution)/shard_map/gather | solution.py:108
  212.8 2.1 reshape.134
  215.0 4.3 %multiply_reduce_fusion = bf16[384,512]{1,0:T(8,128)(2,1)} fusion(f32[384,2,512]{2,1,0:T(2,128)} %reshape.134, f32[384,2]{1,0:T(8,128)S(1)} %copy.49), kind=kLoop, calls=%fused_computation.6 | loop fusion | flops 589824 | bytes 1969152 | tf_op jit(solution)/shard_map/reduce_sum | solution.py:112
  (69 shorter events, 6.6 us)
Async XLA Ops:
  7.2 122.7 %copy-start = (bf16[2048,512]{1,0:T(8,128)(2,1)S(1)}, bf16[2048,512]{1,0:T(8,128)(2,1)}, u32[]{:S(2)}) copy-start(bf16[2048,512]{1,0:T(8,128)(2,1)} %param.17) | copy-start | bytes 6291460
  7.2 7.4 %copy-start.1 = (bf16[96,2048]{1,0:T(8,128)(2,1)S(1)}, bf16[96,2048]{1,0:T(8,128)(2,1)}, u32[]{:S(2)}) copy-start(bf16[96,2048]{1,0:T(8,128)(2,1)} %param.15) | copy-start | bytes 1179652
  7.2 7.6 %copy-start.4 = (f32[2048]{0:T(1024)S(1)}, f32[2048]{0:T(1024)}, u32[]{:S(2)}) copy-start(f32[2048]{0:T(1024)} %param.22) | copy-start | bytes 24580
  7.2 100.9 %all-gather.12.cloned.1.call-start = ((), (), s32[]{:S(2)}) async-start(), calls=%async_computation.5 | async-start | bytes 7864320 | tf_op jit(solution)/shard_map/all_gather | solution.py:77
  62.5 1.0 copy-start.2
  62.5 1.2 copy-start.5
  62.5 67.3 %all-gather.6.cloned.1.call-start = ((), (), s32[]{:S(2)}) async-start(), calls=%async_computation.2 | async-start | bytes 1966080 | tf_op jit(solution)/shard_map/all_gather | solution.py:60
  64.6 95.7 %all-gather.10.cloned.1.call-start = ((), (), s32[]{:S(2)}) async-start(), calls=%async_computation.4 | async-start | bytes 3932160 | tf_op jit(solution)/shard_map/all_gather | solution.py:100
  108.1 3.5 %copy-start.8 = (bf16[1,2048,256]{2,1,0:T(8,128)(2,1)S(1)}, bf16[1,2048,256]{2,1,0:T(8,128)(2,1)}, u32[]{:S(2)}) copy-start(bf16[1,2048,256]{2,1,0:T(8,128)(2,1)} %param.25) | copy-start | bytes 3145732
  111.5 1.9 copy-start.9
  129.9 2.5 %copy-start.6 = (bf16[2048,512]{1,0:T(8,128)(2,1)S(1)}, bf16[2048,512]{1,0:T(8,128)(2,1)}, u32[]{:S(2)}) copy-start(bf16[2048,512]{1,0:T(8,128)(2,1)} %param.19) | copy-start | bytes 6291460
  129.9 2.5 %copy-start.7 = (bf16[384,2048]{1,0:T(8,128)(2,1)S(1)}, bf16[384,2048]{1,0:T(8,128)(2,1)}, u32[]{:S(2)}) copy-start(bf16[384,2048]{1,0:T(8,128)(2,1)} %all-gather.6.cloned.1.call-done) | copy-start | bytes 4718596
  133.4 4.7 %collective-permute-start = (bf16[2,512]{1,0:T(2,128)(2,1)S(1)}, bf16[2,512]{1,0:T(2,128)(2,1)S(1)}, u32[]{:S(2)}, u32[]{:S(2)}) collective-permute-start(bf16[2,512]{1,0:T(2,128)(2,1)S(1)} %slice.44), channel_id=1, source_target_pairs={{0,4},{4,8},{8,12},{12,16},{16,20},{20,24},{24,28},{1,5},{5,9},{9,... | collective-permute-start | bytes 6152 | tf_op jit(solution)/shard_map/ppermute | solution.py:12
  165.5 43.0 %all-to-all-start.1 = ((bf16[8,192,512]{2,1,0:T(8,128)(2,1)}), bf16[8,192,512]{2,1,0:T(8,128)(2,1)}, u32[]{:S(2)}, u32[]{:S(2)}) async-start(bf16[8,192,512]{2,1,0:T(8,128)(2,1)} %bitcast.44), calls=%async_computation.1 | async-start | bytes 3145728 | tf_op jit(solution)/shard_map/all_to_all | solution.py:106
  171.0 24.2 %all-gather.8.cloned.1.call-start = ((), (), s32[]{:S(2)}) async-start(), calls=%async_computation.3 | async-start | bytes 1966080 | tf_op jit(solution)/shard_map/all_gather | solution.py:99
  171.2 4.2 %copy-start.3 = (f32[384,2]{0,1:T(2,128)S(1)}, f32[384,2]{0,1:T(2,128)}, u32[]{:S(2)}) copy-start(f32[384,2]{0,1:T(2,128)} %param.24) | copy-start | bytes 9220
Sparse Core Ops, SparseCore 0:
  62.7 45.3 all-gather.11
  110.2 19.6 all-gather.5
  131.4 28.8 all-gather.9
  175.3 19.8 all-gather.7
